TPU v7x, 256 devices: a whole 4x4x8 slice. The times are simulated.
256 devices in a mesh: fs: 64 (over z, x, core), tp: 4 (over y).
Axes of the slice: x: 4, y: 4, z: 8, core: 2. Of those that a mesh axis runs over, the one named last changes fastest.
Arguments:
- inputs: bfloat16 [65536, 2048], P('fs'), may hold values from -16 to 16
- cotangents: bfloat16 [65536, 3, 1024], P('fs', None, 'tp'), may hold values from -0.0234375 to 0.0234375
- factors: bfloat16 [3, 2048, 256], P(None, 'fs'), may hold values from -13.810679 to 13.810679
- first_moment: float32 [3, 256, 1024], P(None, None, 'tp'), may hold values from -6 to 6
- second_moment: float32 [3, 256, 1024], P(None, None, 'tp'), may hold values from 0.05 to 1
- master: float32 [3, 2048, 1024], P(None, 'fs', 'tp'), may hold values from -0.125 to 0.125
Outputs:
- update_step: float32 [3, 2048, 1024], P(None, 'fs', 'tp')
- new_master: float32 [3, 2048, 1024], P(None, 'fs', 'tp')
- new_copy: bfloat16 [3, 2048, 1024], P(None, None, 'tp')
- new_first: float32 [3, 256, 1024], P(None, None, 'tp')
- new_second: float32 [3, 256, 1024], P(None, None, 'tp')
All inputs are finite; a program needn't handle non-finite values.
Results may differ from a plain program's by a relative error of at most 0.001.
Values may be sent and summed in bfloat16 or wider, within the bound.
A program may use at most 64 MiB of HBM per device.

v0:
```python
import jax
import jax.numpy as jnp
from jax import lax
from jax.sharding import Mesh
from jax.sharding import PartitionSpec as P

D = 2048
MW = 1024
FS = ("fs_0", "fs_1", "fs_2")


beta_first = 0.8
beta_second = 0.9
adam_eps = 1e-08
norm_eps = 1e-06
learning_rate = 0.005


def from_everyone(shard, axis):
    copies = jnp.broadcast_to(shard, (lax.axis_size(axis), *shard.shape))
    return lax.all_to_all(copies, axis, split_axis=0, concat_axis=0, tiled=True)


def laid_out(pieces, dim):
    pieces = jnp.moveaxis(pieces, 0, dim)
    lengths = pieces.shape
    return pieces.reshape(*lengths[:dim], lengths[dim] * lengths[dim + 1], *lengths[dim + 2 :])


def gather_axes(shard, axes, dim):
    far, near = axes
    first = from_everyone(shard, far)
    pieces = jnp.swapaxes(from_everyone(first, near), 0, 1)
    return laid_out(pieces.reshape(-1, *shard.shape), dim)


def padded_to(lines, count):
    spare = -len(lines) % count
    return jnp.pad(lines, [(0, spare)] + [(0, 0)] * (lines.ndim - 1))


def in_blocks(shard, dim, count):
    before, after = (shard.shape[:dim], shard.shape[dim + 1 :])
    return jnp.moveaxis(shard.reshape(*before, count, -1, *after), dim, 0)


def sent_and_summed(shard, axis, dim):
    count = lax.axis_size(axis)
    pieces = lax.all_to_all(in_blocks(shard, dim, count), axis, 0, 0, tiled=True)
    return jnp.sum(pieces, axis=0)


def sum_by_axis(shard, axes, dim):
    far, near = axes
    pieces = in_blocks(shard, dim, lax.axis_size(far))
    nearer = sent_and_summed(pieces, near, dim + 1)
    arrived = lax.all_to_all(nearer, far, split_axis=0, concat_axis=0, tiled=True)
    return arrived.sum(axis=0)


def sum_by_parts(shard, axes):
    lines = shard.reshape(-1, shard.shape[-1])
    padded = padded_to(lines, lax.axis_size(axes[0]) * lax.axis_size(axes[1]))
    whole = gather_axes(sum_by_axis(padded, axes, 0), axes, 0)
    return lax.slice_in_dim(whole, 0, len(lines)).reshape(shard.shape)


def of_everyone(shard, axis):
    everything = from_everyone(shard, axis)
    return jnp.sum(everything, axis=0)


def over_axes(shard, axes):
    far, near = axes
    nearer = of_everyone(shard, near)
    return of_everyone(nearer, far)


def local(inputs, cotangents, factors, first_moment, second_moment, master):
    factor32 = factors.astype(jnp.float32)
    lowered = jnp.einsum(
        "tk,mkr->mtr",
        inputs,
        gather_axes(factors, (("fs_0", "fs_1"), "fs_2"), 1),
        preferred_element_type=jnp.float32,
    )
    cot_wide = cotangents.astype(jnp.float32)
    partial_value = jnp.einsum("mtr,tmc->mrc", lowered, cot_wide, precision=lax.Precision.HIGHEST)
    projected = sum_by_parts(partial_value, (("fs_0", "fs_1"), "fs_2"))
    new_first = beta_first * first_moment + (1.0 - beta_first) * projected
    new_second = beta_second * second_moment + (1.0 - beta_second) * projected * projected
    normed = new_first / (jnp.sqrt(new_second) + adam_eps)
    update = jnp.einsum("mdr,mrc->mdc", factor32, normed, precision=lax.Precision.HIGHEST)
    squares = over_axes(jnp.sum(update * update, axis=(1, 2)), (("fs_0", "fs_1"), ("fs_2", "tp")))
    root_mean = jnp.sqrt(squares / (D * MW) + norm_eps)
    update_step = update / root_mean[:, None, None]
    new_master = master - learning_rate * update_step
    new_copy = gather_axes(new_master.astype(jnp.bfloat16), (("fs_0", "fs_1"), "fs_2"), 1)
    return (update_step, new_master, new_copy, new_first, new_second)


def solution(mesh):
    torus = Mesh(mesh.devices.reshape(8, 4, 2, mesh.shape["tp"]), ("fs_0", "fs_1", "fs_2", "tp"))
    return jax.shard_map(
        local,
        mesh=torus,
        in_specs=(
            P(FS, None),
            P(FS, None, "tp"),
            P(None, FS, None),
            P(None, None, "tp"),
            P(None, None, "tp"),
            P(None, FS, "tp"),
        ),
        out_specs=(
            P(None, FS, "tp"),
            P(None, FS, "tp"),
            P(None, None, "tp"),
            P(None, None, "tp"),
            P(None, None, "tp"),
        ),
        check_vma=False,
    )
```

profile of v0, /device:TPU:1, one launch (start us, length us, event | category | flops | bytes accessed | tf_op | source)
XLA Modules:
  0.0 202.5 jit_solution(17605297059751023663)
XLA Ops:
  0.6 1.1 broadcast_in_dim.25
  1.8 50.3 %all_to_all.52 = bf16[32,3,32,256]{3,2,1,0:T(8,128)(2,1)S(1)} all-to-all(bf16[32,3,32,256]{3,2,1,0:T(8,128)(2,1)S(1)} %broadcast_in_dim.25), channel_id=1, replica_groups=mesh['fs_0'=8,'fs_1'=4,'fs_2'=2,'tp'=4] {'fs_0','fs_1'}, dimensions={0} | all-to-all | bytes 3145728 | tf_op jit(solution)/shard_map/all_to_all | solution.py:21
  52.0 0.4 broadcast_in_dim.26
  52.4 8.6 %all_to_all.53 = bf16[2,32,3,32,256]{4,3,2,1,0:T(8,128)(2,1)S(1)} all-to-all(bf16[2,32,3,32,256]{4,3,2,1,0:T(8,128)(2,1)S(1)} %broadcast_in_dim.26), channel_id=1, replica_groups=mesh['fs_0'=8,'fs_1'=4,'fs_2'=2,'tp'=4] {'fs_2'}, dimensions={0} | all-to-all | bytes 6291456 | tf_op jit(solution)/shard_map/all_to_all | solution.py:21
  61.1 0.4 copy.74
  61.5 0.4 copy.75
  61.9 1.8 copy-done.5
  63.7 3.5 %fusion = f32[3,256,1024]{2,1,0:T(8,128)S(1)} fusion(bf16[3,2048,256]{2,1,0:T(8,128)(2,1)S(1)} %bitcast.29, bf16[1024,2048]{1,0:T(8,128)(2,1)S(1)} %copy-done.5), kind=kOutput, calls=%fused_computation | convolution fusion | flops 3221225472 | bytes 10485760 | tf_op jit(solution)/shard_map/tk,mkr->mtr/dot_general | solution.py:81
  67.2 1.6 fusion.7
  68.8 0.1 reshape_reshape.3
  68.9 0.5 copy.77
  69.3 4.4 %all_to_all.54 = f32[2,32,12,256]{3,1,2,0:T(8,128)S(1)} all-to-all(f32[2,32,12,256]{3,1,2,0:T(8,128)S(1)} %copy.77), channel_id=1, replica_groups=mesh['fs_0'=8,'fs_1'=4,'fs_2'=2,'tp'=4] {'fs_2'}, dimensions={0} | all-to-all | bytes 1572864 | tf_op jit(solution)/shard_map/all_to_all | solution.py:49
  73.7 0.2 copy.78
  74.0 20.6 %all_to_all.55 = f32[32,12,256]{2,1,0:T(8,128)S(1)} all-to-all(f32[32,12,256]{2,1,0:T(8,128)S(1)} %copy.78), channel_id=1, replica_groups=mesh['fs_0'=8,'fs_1'=4,'fs_2'=2,'tp'=4] {'fs_0','fs_1'}, dimensions={0} | all-to-all | bytes 786432 | tf_op jit(solution)/shard_map/all_to_all | solution.py:57
  94.7 20.0 %all_to_all.56 = f32[32,12,256]{2,1,0:T(8,128)S(1)} all-to-all(f32[32,12,256]{2,1,0:T(8,128)S(1)} %broadcast_in_dim.27), channel_id=1, replica_groups=mesh['fs_0'=8,'fs_1'=4,'fs_2'=2,'tp'=4] {'fs_0','fs_1'}, dimensions={0} | all-to-all | bytes 786432 | tf_op jit(solution)/shard_map/all_to_all | solution.py:21
  114.7 0.2 copy.79
  115.0 7.6 %all_to_all.57 = f32[2,32,12,256]{3,1,2,0:T(8,128)S(1)} all-to-all(f32[2,32,12,256]{3,1,2,0:T(8,128)S(1)} %broadcast_in_dim.28), channel_id=1, replica_groups=mesh['fs_0'=8,'fs_1'=4,'fs_2'=2,'tp'=4] {'fs_2'}, dimensions={0} | all-to-all | bytes 1572864 | tf_op jit(solution)/shard_map/all_to_all | solution.py:21
  122.6 0.5 copy.80
  123.0 0.1 reshape_reshape_reshape.3
  123.1 1.6 fusion.2
  124.8 0.9 copy-done.2
  125.7 0.8 multiply_reduce_fusion
  126.4 9.2 %all_to_all.58 = f32[8,1,3]{2,1,0:T(1,128)S(1)} all-to-all(f32[8,1,3]{2,1,0:T(1,128)S(1)} %broadcast_in_dim.29), channel_id=1, replica_groups=mesh['fs_0'=8,'fs_1'=4,'fs_2'=2,'tp'=4] {'fs_2','tp'}, dimensions={0} | all-to-all | bytes 192 | tf_op jit(solution)/shard_map/all_to_all | solution.py:21
  135.7 12.7 %all_to_all.59 = f32[32,1,3]{2,1,0:T(1,128)S(1)} all-to-all(f32[32,1,3]{2,1,0:T(1,128)S(1)} %broadcast_in_dim.30), channel_id=1, replica_groups=mesh['fs_0'=8,'fs_1'=4,'fs_2'=2,'tp'=4] {'fs_0','fs_1'}, dimensions={0} | all-to-all | bytes 768 | tf_op jit(solution)/shard_map/all_to_all | solution.py:21
  148.4 0.8 fusion.6
  149.2 0.2 broadcast_in_dim.31
  149.4 40.6 %all_to_all.60 = bf16[32,3,32,256]{3,2,1,0:T(8,128)(2,1)S(1)} all-to-all(bf16[32,3,32,256]{3,2,1,0:T(8,128)(2,1)S(1)} %broadcast_in_dim.31), channel_id=1, replica_groups=mesh['fs_0'=8,'fs_1'=4,'fs_2'=2,'tp'=4] {'fs_0','fs_1'}, dimensions={0} | all-to-all | bytes 3145728 | tf_op jit(solution)/shard_map/all_to_all | solution.py:21
  190.0 0.1 copy.83
  190.1 0.4 broadcast_in_dim.32
  190.5 9.5 %all_to_all.61 = bf16[2,32,3,32,256]{4,3,1,2,0:T(8,128)(2,1)S(1)} all-to-all(bf16[2,32,3,32,256]{4,3,1,2,0:T(8,128)(2,1)S(1)} %broadcast_in_dim.32), channel_id=1, replica_groups=mesh['fs_0'=8,'fs_1'=4,'fs_2'=2,'tp'=4] {'fs_2'}, dimensions={0} | all-to-all | bytes 6291456 | tf_op jit(solution)/shard_map/all_to_all | solution.py:21
  200.0 0.4 copy.84
  200.4 2.1 %copy.85 = bf16[3,64,32,256]{3,2,1,0:T(8,128)(2,1)} copy(bf16[3,64,32,256]{3,2,0,1:T(8,128)(2,1)S(1)} %bitcast.25) | data formatting | bytes 6291456 | tf_op jit(solution)/shard_map/transpose | solution.py:25
  (19 shorter events, 0.4 us)
Async XLA Ops:
  0.6 66.5 %copy-start = (bf16[1024,3,256]{2,0,1:T(8,128)(2,1)S(1)}, bf16[1024,3,256]{2,0,1:T(8,128)(2,1)}, u32[]{:S(2)}) copy-start(bf16[1024,3,256]{2,0,1:T(8,128)(2,1)} %param.7) | copy-start | bytes 4718596
  61.5 2.2 %copy-start.5 = (bf16[1024,2048]{1,0:T(8,128)(2,1)S(1)}, bf16[1024,2048]{1,0:T(8,128)(2,1)}, u32[]{:S(2)}) copy-start(bf16[1024,2048]{1,0:T(8,128)(2,1)} %param.6) | copy-start | bytes 12582916
  123.0 2.6 %copy-start.4 = (bf16[3,32,256]{2,1,0:T(8,128)(2,1)S(1)}, bf16[3,32,256]{2,1,0:T(8,128)(2,1)}, u32[]{:S(2)}) copy-start(bf16[3,32,256]{2,1,0:T(8,128)(2,1)} %param.8) | copy-start | bytes 147460
  123.1 25.3 %copy-start.3 = (f32[3,32,256]{2,1,0:T(8,128)S(1)}, f32[3,32,256]{2,1,0:T(8,128)}, u32[]{:S(2)}) copy-start(f32[3,32,256]{2,1,0:T(8,128)} %param.11) | copy-start | bytes 294916
  124.8 0.9 copy-start.2
  124.8 65.2 %copy-start.1 = (f32[3,256,256]{2,1,0:T(8,128)}, f32[3,256,256]{2,1,0:T(8,128)S(1)}, u32[]{:S(2)}) copy-start(f32[3,256,256]{2,1,0:T(8,128)S(1)} %get-tuple-element.8) | copy-start | bytes 2359300
where the time goes:
time: 203 us
  blocking collectives  183 us (90%)
  local copies, waits for them, and re-layouts  10 us (5%)
  matrix products  5.77 us (3%)
  other arithmetic  2.59 us (1%)
    all_to_all x8, blocking collectives, from_everyone(): return lax.all_to_all(copies, axis, split_axis=0, concat_axis=0, tiled=True)  158 us
    all_to_all x1, blocking collectives, sum_by_axis(): lax.all_to_all(nearer, far, split_axis=0, concat_axis=0, tiled=True)  20.6 us
    all_to_all x1, blocking collectives, sent_and_summed(): lax.all_to_all(in_blocks(shard, dim, count), axis, 0, 0, tiled=True)  4.36 us

commit v1 on v0

v1 whole, which is shorter than its diff:
```python
import jax
import jax.numpy as jnp
from jax import lax
from jax.experimental import pallas as pl
from jax.experimental.pallas import tpu as pltpu
from jax.sharding import Mesh
from jax.sharding import PartitionSpec as P

D = 2048
MW = 1024
BF = jnp.bfloat16
F32 = jnp.float32
MESH = pl.DeviceIdType.MESH

beta_first = 0.8
beta_second = 0.9
adam_eps = 1e-08
norm_eps = 1e-06
learning_rate = 0.005

NZ, NX = 8, 4
GATHER_COPIES = 48


class Gather:
    def __init__(self, pos, first0, first1, ssem, rsem):
        self.z, self.x, self.c, self.y = pos
        self.b0, self.b1 = first0, first1
        self.ssem, self.rsem = ssem, rsem
        self.count = 0
        self.sent = []

    def at(self, dz=0, dx=0, other=False):
        z = lax.rem(self.z + (dz + NZ), NZ)
        x = lax.rem(self.x + (dx + NX), NX)
        return (z, x, 1 - self.c if other else self.c, self.y)

    def zof(self, dz):
        return lax.rem(self.z + (dz + NZ), NZ)

    def xof(self, dx):
        return lax.rem(self.x + (dx + NX), NX)

    def send(self, ref, target):
        k = self.count
        self.count += 1
        copy = pltpu.make_async_remote_copy(
            src_ref=ref, dst_ref=ref, send_sem=self.ssem.at[k], recv_sem=self.rsem.at[k], device_id=target, device_id_type=MESH
        )
        copy.start()
        self.sent.append(copy)
        return copy

    def pair(self, ref):
        self.pairs.append(self.send(ref, self.at(other=True)))

    def blk(self, dz, part=None):
        if part is None:
            return self.b0.at[self.c, self.zof(dz)]
        return self.b0.at[self.c, self.zof(dz), pl.ds(2 * part, 2)]

    def col(self, dx, part=None):
        if part is None:
            return self.b1.at[self.c, self.xof(dx)]
        return self.b1.at[self.c, self.xof(dx), pl.ds(4 * part, 4)]

    def stages(self):
        self.pairs = []
        c, z, x = self.c, self.z, self.x
        own0, own1 = self.b0.at[c, z, x], self.b1.at[c, x, z]
        near = [self.send(own0, self.at(dx=dx)) for dx in (1, -1, 2)]
        far = [self.send(own1, self.at(dz=dz)) for dz in (1, -1, 2, -2, 3, -3, 4)]
        yield
        for k in near:
            k.wait_recv()
        right = self.send(self.blk(0), self.at(dz=1))
        left = self.send(self.blk(0), self.at(dz=-1))
        self.pair(self.blk(0))
        yield
        for k in far:
            k.wait_recv()
        east = self.send(self.col(0), self.at(dx=1))
        west = self.send(self.col(0), self.at(dx=-1))
        self.pair(self.col(0))
        yield
        for step in (1, 2):
            right.wait_recv()
            left.wait_recv()
            right = self.send(self.blk(-step), self.at(dz=1))
            left = self.send(self.blk(step), self.at(dz=-1))
            self.pair(self.blk(-step))
            self.pair(self.blk(step))
            yield
            if step == 1:
                east.wait_recv()
                west.wait_recv()
                east = self.send(self.col(-1, 0), self.at(dx=1))
                west = self.send(self.col(1, 1), self.at(dx=-1))
                self.pair(self.col(-1))
                self.pair(self.col(1))
                yield
        right.wait_recv()
        left.wait_recv()
        right = self.send(self.blk(-3, 0), self.at(dz=1))
        left = self.send(self.blk(3, 1), self.at(dz=-1))
        self.pair(self.blk(-3))
        self.pair(self.blk(3))
        yield
        east.wait_recv()
        west.wait_recv()
        self.pair(self.col(2))
        yield
        right.wait_recv()
        left.wait_recv()
        self.pair(self.blk(4))
        yield
        for k in self.pairs:
            k.wait_recv()

    def drain(self):
        for k in self.sent:
            k.wait_send()


def split(value):
    high = value.astype(BF)
    return high, (value - high.astype(F32)).astype(BF)


def dot(a, b):
    return lax.dot_general(a, b, (((1,), (0,)), ((), ())), preferred_element_type=F32)


def dot_first(a, b):
    return lax.dot_general(a, b, (((0,), (0,)), ((), ())), preferred_element_type=F32)


def chunk_of(b0, b1, z, m):
    pieces = []
    for x in range(NX):
        for c in range(2):
            pieces.append(b0[c, z, x, m])
            pieces.append(b1[c, x, z, m])
    return jnp.concatenate(pieces, axis=0)


def kernel(
    inputs, cots, factors, first, second, master,
    out_step, out_master, out_copy, out_first, out_second,
    xin, cin, f0, f1, m0, m1, ghi, glo, fm, sm, um, own_f32, own_step, own_new, copy_v,
    pa, pb, ca, cb, sa, sb, rxa, rzb, ta, tb, rza, rxb, ga, gb, nhi, nlo, squares,
    lsem, osem, fs_sem, fr_sem, ms_sem, mr_sem, bs_sem, br_sem,
):
    z, x, c, y = (lax.axis_index(a) for a in ("z", "x", "c", "y"))
    pos = (z, x, c, y)

    local = []

    def load(src, dst):
        k = pltpu.make_async_copy(src, dst, lsem.at[len(local)])
        k.start()
        local.append(k)
        return k

    fl = [
        load(factors.at[:, pl.ds(0, 16), :], f0.at[c, z, x]),
        load(factors.at[:, pl.ds(16, 16), :], f1.at[c, x, z]),
    ]
    xl = load(inputs, xin)
    cl = load(cots, cin)
    ml = [
        load(master.at[:, pl.ds(0, 16), :], m0.at[c, z, x]),
        load(master.at[:, pl.ds(16, 16), :], m1.at[c, x, z]),
    ]
    el = [load(first, fm), load(second, sm), load(master, own_f32)]

    barrier = pltpu.get_barrier_semaphore()
    peers = []
    for dz in range(1, NZ):
        peers.append((lax.rem(z + dz, NZ), x, c, y))
    for dx in range(1, NX):
        peers.append((z, lax.rem(x + dx, NX), c, y))
    for dy in range(1, 4):
        peers.append((z, x, c, lax.rem(y + dy, 4)))
    peers.append((z, x, 1 - c, y))
    for peer in peers:
        pl.semaphore_signal(barrier, inc=1, device_id=peer, device_id_type=MESH)
    for k in fl:
        k.wait()
    pl.semaphore_wait(barrier, len(peers))

    def gradient(lo, hi):
        def body(zz, _):
            xs = xin[:, pl.ds(pl.multiple_of(zz * 256, 256), 256)]
            for m in range(3):
                g_hi, g_lo = split(dot_first(xs, cin[m]))
                ghi[m, zz] = g_hi
                glo[m, zz] = g_lo
            return 0
        lax.fori_loop(lo, hi, body, 0)

    fg = Gather(pos, f0, f1, fs_sem, fr_sem)
    fst = fg.stages()
    next(fst)
    xl.wait()
    cl.wait()
    gradient(0, 4)
    next(fst)
    gradient(4, 8)
    for _ in fst:
        pass

    mg = Gather(pos, m0, m1, ms_sem, mr_sem)
    mst = mg.stages()
    for k in ml:
        k.wait()
    next(mst)

    for m in range(3):
        def body(zz, acc):
            f = chunk_of(f0, f1, zz, m)
            return acc + dot_first(f, ghi[m, zz]) + dot_first(f, glo[m, zz])
        acc = lax.fori_loop(0, NZ, body, jnp.zeros((256, 256), F32))
        for half in range(2):
            part = acc[:, half * 128:(half + 1) * 128]
            if m < 2:
                for xx in range(NX):
                    pa[half, xx, m] = part[xx * 64:(xx + 1) * 64]
            else:
                for zz in range(NZ):
                    pb[half, zz] = part[zz * 32:(zz + 1) * 32]

    started = []

    def send(src, dst, target):
        k = len(started)
        copy = pltpu.make_async_remote_copy(
            src_ref=src, dst_ref=dst, send_sem=bs_sem.at[k], recv_sem=br_sem.at[k], device_id=target, device_id_type=MESH
        )
        copy.start()
        started.append(copy)
        return copy

    def got(copies):
        for k in copies:
            k.wait_recv()

    partner = (z, x, 1 - c, y)

    def zpeer(dz):
        return lax.rem(z + (dz + NZ), NZ)

    def xpeer(dx):
        return lax.rem(x + (dx + NX), NX)

    zorder = (4, 3, -3, 2, -2, 1, -1)
    xorder = (2, 1, -1)

    k1 = send(pb.at[1 - c], cb, partner)
    k2 = send(pa.at[1 - c], ca, partner)
    got([k1])
    sb[...] = pb[c] + cb[...]
    b1 = [send(sb.at[zpeer(dz)], rzb.at[i], (zpeer(dz), x, c, y)) for i, dz in enumerate(zorder)]
    got([k2])
    sa[...] = pa[c] + ca[...]
    a1 = [send(sa.at[xpeer(dx)], rxa.at[i], (z, xpeer(dx), c, y)) for i, dx in enumerate(xorder)]
    next(mst)
    got(a1)
    for m in range(2):
        tot = sa[x, m]
        for i in range(3):
            tot = tot + rxa[i, m]
        for zz in range(NZ):
            ta[zz, m] = tot[zz * 8:(zz + 1) * 8]
    a2 = [send(ta.at[zpeer(dz)], rza.at[i], (zpeer(dz), x, c, y)) for i, dz in enumerate(zorder)]
    got(b1)
    tot = sb[z]
    for i in range(7):
        tot = tot + rzb[i]
    for xx in range(NX):
        tb[xx] = tot[xx * 8:(xx + 1) * 8]
    b2 = [send(tb.at[xpeer(dx)], rxb.at[i], (z, xpeer(dx), c, y)) for i, dx in enumerate(xorder)]
    next(mst)
    got(b2)
    tot = tb[x]
    for i in range(3):
        tot = tot + rxb[i]
    gb[c, z, x] = tot
    b3 = [send(gb.at[c, z, x], gb.at[c, z, x], (z, xpeer(dx), c, y)) for dx in xorder]
    got(a2)
    tot = ta[z]
    for i in range(7):
        tot = tot + rza[i]
    ga[c, x, z] = tot
    a3 = [send(ga.at[c, x, z], ga.at[c, x, z], (zpeer(dz), x, c, y)) for dz in zorder]
    got(b3)
    b4 = [send(gb.at[c, z], gb.at[c, z], (zpeer(dz), x, c, y)) for dz in zorder]
    next(mst)
    got(a3)
    a4 = [send(ga.at[c, x], ga.at[c, x], (z, xpeer(dx), c, y)) for dx in xorder]
    next(mst)
    got(a4)
    ka = send(ga.at[c], ga.at[c], partner)
    got(b4)
    kb = send(gb.at[c], gb.at[c], partner)
    next(mst)
    got([ka, kb])

    for k in el:
        k.wait()
    outs = []

    def store(src, dst):
        k = pltpu.make_async_copy(src, dst, osem.at[len(outs)])
        k.start()
        outs.append(k)

    for m in range(3):
        for half in range(2):
            cols = slice(half * 128, (half + 1) * 128)
            if m < 2:
                proj = jnp.concatenate([ga[half, xx, zz, m] for xx in range(NX) for zz in range(NZ)], axis=0)
            else:
                proj = jnp.concatenate([gb[half, zz, xx] for zz in range(NZ) for xx in range(NX)], axis=0)
            nf = beta_first * fm[m, :, cols] + (1.0 - beta_first) * proj
            ns = beta_second * sm[m, :, cols] + (1.0 - beta_second) * proj * proj
            fm[m, :, cols] = nf
            sm[m, :, cols] = ns
            hi, lo = split(nf / (jnp.sqrt(ns) + adam_eps))
            nhi[m, :, cols] = hi
            nlo[m, :, cols] = lo
    store(fm, out_first)
    store(sm, out_second)
    next(mst)
    ys = []
    for m in range(3):
        def body(zz, acc):
            f = chunk_of(f0, f1, zz, m)
            u = dot(f, nhi[m]) + dot(f, nlo[m])
            um[m, pl.ds(pl.multiple_of(zz * 256, 256), 256), :] = u
            uu = (u * u).reshape(32, 8, 256)
            uu = jnp.sum(uu, axis=0)
            return acc + uu[:, :128] + uu[:, 128:]
        squares[y, m] = lax.fori_loop(0, NZ, body, jnp.zeros((8, 128), F32))
        ys += [send(squares.at[y, m], squares.at[y, m], (z, x, c, lax.rem(y + dy, 4))) for dy in (1, 2, 3)]
        if m < 2:
            next(mst)
    for _ in mst:
        pass
    got(ys)

    rows = pl.multiple_of(z * 256 + x * 64 + c * 32, 32)
    for m in range(3):
        tot = squares[0, m]
        for j in range(1, 4):
            tot = tot + squares[j, m]
        inv = 1.0 / jnp.sqrt(jnp.sum(tot, keepdims=True) / (D * MW) + norm_eps)
        step = um[m, pl.ds(rows, 32), :] * inv
        own_step[m] = step
        own_new[m] = own_f32[m] - learning_rate * step

        def body(zz, _):
            at = pl.ds(pl.multiple_of(zz * 256, 256), 256)
            copy_v[m, at, :] = (chunk_of(m0, m1, zz, m) - learning_rate * (um[m, at, :] * inv)).astype(BF)
            return 0
        lax.fori_loop(0, NZ, body, 0)
        store(copy_v.at[m], out_copy.at[m])
    store(own_step, out_step)
    store(own_new, out_master)
    fg.drain()
    mg.drain()
    for k in started:
        k.wait_send()
    for k in outs:
        k.wait()


def local(inputs, cotangents, factors, first_moment, second_moment, master):
    cots = jnp.transpose(cotangents, (1, 0, 2))
    anyspace = pl.BlockSpec(memory_space=pl.ANY)
    V = pltpu.VMEM
    dma = pltpu.SemaphoreType.DMA
    return pl.pallas_call(
        kernel,
        out_shape=(
            jax.ShapeDtypeStruct((3, 32, 256), F32),
            jax.ShapeDtypeStruct((3, 32, 256), F32),
            jax.ShapeDtypeStruct((3, D, 256), BF),
            jax.ShapeDtypeStruct((3, 256, 256), F32),
            jax.ShapeDtypeStruct((3, 256, 256), F32),
        ),
        in_specs=[anyspace] * 6,
        out_specs=(anyspace,) * 5,
        scratch_shapes=[
            V((1024, 2048), BF), V((3, 1024, 256), BF),
            V((2, NZ, NX, 3, 16, 256), BF), V((2, NX, NZ, 3, 16, 256), BF),
            V((2, NZ, NX, 3, 16, 256), F32), V((2, NX, NZ, 3, 16, 256), F32),
            V((3, NZ, 256, 256), BF), V((3, NZ, 256, 256), BF),
            V((3, 256, 256), F32), V((3, 256, 256), F32), V((3, D, 256), F32),
            V((3, 32, 256), F32), V((3, 32, 256), F32), V((3, 32, 256), F32), V((3, D, 256), BF),
            V((2, NX, 2, 64, 128), F32), V((2, NZ, 32, 128), F32),
            V((NX, 2, 64, 128), F32), V((NZ, 32, 128), F32),
            V((NX, 2, 64, 128), F32), V((NZ, 32, 128), F32),
            V((3, 2, 64, 128), F32), V((7, 32, 128), F32),
            V((NZ, 2, 8, 128), F32), V((NX, 8, 128), F32),
            V((7, 2, 8, 128), F32), V((3, 8, 128), F32),
            V((2, NX, NZ, 2, 8, 128), F32), V((2, NZ, NX, 8, 128), F32),
            V((3, 256, 256), BF), V((3, 256, 256), BF), V((4, 3, 8, 128), F32),
            dma((16,)), dma((8,)),
            dma((GATHER_COPIES,)), dma((GATHER_COPIES,)), dma((GATHER_COPIES,)), dma((GATHER_COPIES,)),
            dma((64,)), dma((64,)),
        ],
        compiler_params=pltpu.CompilerParams(collective_id=0, has_side_effects=True, vmem_limit_bytes=60 * 1024 * 1024),
        name="update",
    )(inputs, cots, factors, first_moment, second_moment, master)


def solution(mesh):
    torus = Mesh(mesh.devices.reshape(NZ, NX, 2, mesh.shape["tp"]), ("z", "x", "c", "y"))
    fs = ("z", "x", "c")
    return jax.shard_map(
        local,
        mesh=torus,
        in_specs=(
            P(fs, None),
            P(fs, None, "y"),
            P(None, fs, None),
            P(None, None, "y"),
            P(None, None, "y"),
            P(None, fs, "y"),
        ),
        out_specs=(
            P(None, fs, "y"),
            P(None, fs, "y"),
            P(None, None, "y"),
            P(None, None, "y"),
            P(None, None, "y"),
        ),
        check_vma=False,
    )
```

time: 203 us -> 96.6 us (0.48)
  blocking collectives: 183 us -> 0 us
  Pallas kernels: 0 us -> 86.5 us
  matrix products: 5.77 us -> 0 us
  other arithmetic: 2.59 us -> 0 us
    all_to_all x10 -> x0, blocking collectives: 183 us -> none  [the longest x8 158 us: from_everyone(): return lax.all_to_all(copies, axis, split_axis=0, concat_axis=0, tiled=True)]
    pallas_call x0 -> x1, Pallas kernels: none -> 86.5 us  [local(): pl.pallas_call(kernel, out_shape=(jax.ShapeDtypeStruct((3, 32, 256), F32)...]
    unnamed x12 -> x9, local copies, waits for them, and re-layouts: 2.68 us -> 8.72 us
    dot_general x3 -> x0, matrix products: 5.77 us -> none  [the longest x1 3.46 us: local(): jnp.einsum('tk,mkr->mtr', inputs, gather_axes(factors, (('fs_0', 'fs_1'),...]
    transpose x4 -> x0, local copies, waits for them, and re-layouts: 3.39 us -> none  [the longest x2 2.45 us: laid_out(): pieces = jnp.moveaxis(pieces, 0, dim)]
    broadcast_in_dim x8 -> x0, local copies, waits for them, and re-layouts: 2.29 us -> none  [from_everyone(): copies = jnp.broadcast_to(shard, (lax.axis_size(axis), *shard.shape))]
where the time goes in v1:
time: 96.6 us; the launch traced here: 95.8 us
  Pallas kernels  86.5 us (90%)
  local copies, waits for them, and re-layouts  8.72 us (9%)
    pallas_call x1, Pallas kernels, local(): pl.pallas_call(kernel, out_shape=(jax.ShapeDtypeStruct((3, 32, 256), F32)...  86.5 us
    unnamed x9, local copies, waits for them, and re-layouts  8.72 us

profile of v1, /device:TPU:1, one launch (start us, length us, event | category | flops | bytes accessed | tf_op | source)
XLA Modules:
  0.0 95.8 jit_solution(13804319368084858778)
XLA Ops:
  0.6 86.5 %update.1 = (f32[3,32,256]{2,1,0:T(8,128)}, f32[3,32,256]{2,1,0:T(8,128)}, bf16[3,2048,256]{2,1,0:T(8,128)(2,1)}, f32[3,256,256]{2,1,0:T(8,128)}, f32[3,256,256]{2,1,0:T(8,128)}) custom-call(bf16[1024,2048]{1,0:T(8,128)(2,1)} %inputs.1, bf16[3,1024,256]{2,1,0:T(8,128)(2,1)} %bitcast.1, bf16[3,32,256]{2,1,0:T(8,128)(2,1)} %factors.1, f32[3,256,256]{2,1,0:T(8,128)} %first.1, ...), custom_call_target="tpu_custom_call" | custom-call | tf_op jit(solution)/shard_map/update/pallas_call | solution.py:383
  87.1 1.5 %copy.16 = f32[3,32,256]{2,1,0:T(8,128)} copy(f32[3,32,256]{2,1,0:T(8,128)} %get-tuple-element.10) | data formatting | bytes 196608
  88.6 1.5 %copy.17 = f32[3,32,256]{2,1,0:T(8,128)} copy(f32[3,32,256]{2,1,0:T(8,128)} %get-tuple-element.11) | data formatting | bytes 196608
  90.2 0.0 copy-start.1
  90.2 0.0 copy-start
  90.2 3.9 %copy.18 = bf16[3,2048,256]{2,1,0:T(8,128)(2,1)} copy(bf16[3,2048,256]{2,1,0:T(8,128)(2,1)} %get-tuple-element.12) | data formatting | bytes 6291456
  94.1 0.0 copy-done.1
  94.1 0.9 copy.19
  94.9 0.0 copy-done
  94.9 0.9 copy.20
Async XLA Ops:
  90.2 3.9 %copy-start.1 = (f32[3,256,256]{2,1,0:T(8,128)S(1)}, f32[3,256,256]{2,1,0:T(8,128)}, u32[]{:S(2)}) copy-start(f32[3,256,256]{2,1,0:T(8,128)} %get-tuple-element.13) | copy-start | bytes 2359300
  90.2 4.8 %copy-start = (f32[3,256,256]{2,1,0:T(8,128)S(1)}, f32[3,256,256]{2,1,0:T(8,128)}, u32[]{:S(2)}) copy-start(f32[3,256,256]{2,1,0:T(8,128)} %get-tuple-element.14) | copy-start | bytes 2359300

commit v2 on v1

v2 whole, which is shorter than its diff:
```python
import jax
import jax.numpy as jnp
from jax import lax
from jax.experimental import pallas as pl
from jax.experimental.pallas import tpu as pltpu
from jax.sharding import Mesh
from jax.sharding import PartitionSpec as P

D = 2048
MW = 1024
BF = jnp.bfloat16
F32 = jnp.float32
MESH = pl.DeviceIdType.MESH

beta_first = 0.8
beta_second = 0.9
adam_eps = 1e-08
norm_eps = 1e-06
learning_rate = 0.005

NZ, NX = 8, 4
GATHER_COPIES = 96
ORDER = (2, 0, 1)


class Gather:
    def __init__(self, pos, whole, ssem, rsem, flip):
        self.z, self.x, self.c, self.y = pos
        self.b = whole
        self.ssem, self.rsem = ssem, rsem
        self.flip = flip
        self.sent = []
        self.waiting = {}
        self.pairs = {m: [] for m in range(3)}
        self.rest = []

    def zof(self, dz):
        return lax.rem(self.z + (dz + NZ), NZ)

    def xof(self, dx):
        return lax.rem(self.x + (dx + NX), NX)

    def send(self, ref, dz=0, dx=0, other=False, key=None):
        k = len(self.sent)
        copy = pltpu.make_async_remote_copy(
            src_ref=ref, dst_ref=ref, send_sem=self.ssem.at[k], recv_sem=self.rsem.at[k],
            device_id=(self.zof(dz), self.xof(dx), 1 - self.c if other else self.c, self.y), device_id_type=MESH,
        )
        copy.start()
        self.sent.append(copy)
        if key is not None:
            self.waiting[key] = copy
        return copy

    def got(self, key):
        self.waiting.pop(key).wait_recv()

    def blk(self, dz, m, part=None):
        xs = slice(None) if part is None else pl.ds(2 * part, 2)
        return self.b.at[m, self.zof(dz), xs, self.c, 0]

    def one(self, dz, dx):
        return self.b.at[:, self.zof(dz), self.xof(dx), self.c, 1]

    def start(self):
        own = self.b.at[:, self.z, self.x, self.c, 0]
        for dx in (2, 1, -1):
            self.send(own, dx=dx, key=("near", dx))
        own = self.one(0, 0)
        self.send(own, dz=1, key=("far", 1, -1))
        self.send(own, dz=-1, key=("far", 1, 1))
        self.cross_start(0)

    def cross_start(self, dz):
        self.send(self.one(dz, 0), dx=1, key=("cross", dz, -1))
        self.send(self.one(dz, 0), dx=-1, key=("cross", dz, 1))

    def near(self):
        for dx in (2, 1, -1):
            self.got(("near", dx))
        for m in ORDER:
            self.send(self.blk(0, m), dz=1, key=("ring", 1, m, -1))
            self.send(self.blk(0, m), dz=-1, key=("ring", 1, m, 1))
        for m in ORDER:
            self.pairs[m].append(self.send(self.blk(0, m), other=True))

    def ring(self, k, m):
        for side in (-1, 1):
            self.got(("ring", k, m, side))
            if k < 4:
                part = None if k < 3 else (0 if side < 0 else 1)
                self.send(self.blk(side * k, m, part), dz=-side, key=("ring", k + 1, m, side))
        if k < 4:
            for side in (-1, 1):
                self.pairs[m].append(self.send(self.blk(side * k, m), other=True))
        else:
            self.pairs[m].append(self.send(self.blk(4, m), other=True))

    def far(self, k):
        for side in (-1, 1) if k < 4 else (self.flip,):
            self.got(("far", k, side))
            if k < 3 or (k == 3 and side == self.flip):
                self.send(self.one(side * k, 0), dz=-side, key=("far", k + 1, side))
            self.cross_start(side * k)

    def cross(self, k):
        for dz in ((k, -k) if 0 < k < 4 else (self.flip * k,)):
            side = self.flip if dz % 2 else -self.flip
            for dx in (-1, 1):
                self.got(("cross", dz, dx))
            self.send(self.one(dz, side), dx=-side, key=("cross2", dz))

    def cross2(self, k):
        for dz in ((k, -k) if 0 < k < 4 else (self.flip * k,)):
            self.got(("cross2", dz))
            self.rest.append(self.send(self.b.at[:, self.zof(dz), :, self.c, 1], other=True))

    def paired(self, m):
        for k in self.pairs[m] + self.rest:
            k.wait_recv()
        self.rest = []

    def drain(self):
        for k in self.sent:
            k.wait_send()


def split(value):
    high = value.astype(BF)
    return high, (value - high.astype(F32)).astype(BF)


FLOOR = 2.0 ** -124


def coded(value):
    t = jnp.abs(value) * 8.0
    t = t * t
    t = t * t
    t = t * t * 2.0 ** 60
    t = jnp.maximum(t * t, FLOOR)
    return jnp.where(value < 0, -t, t).astype(BF)


def decoded(code):
    t = code.astype(F32)
    size = jnp.abs(t)
    root = lax.rsqrt(lax.rsqrt(lax.rsqrt(lax.rsqrt(size)))) * (2.0 ** -7.5 / 8.0)
    root = jnp.where(size > FLOOR, root, 0.0)
    return jnp.where(t < 0, -root, root)


def dot(a, b):
    return lax.dot_general(a, b, (((1,), (0,)), ((), ())), preferred_element_type=F32)


def kernel(
    inputs, cots, factors, first, second, master,
    own_step, own_new, copy_v, fm, sm,
    xin, cin, ct, fw, mw, wide, gt, um, own_f32,
    pa, pb, ca, cb, sa, sb, rxa, rzb, ta, tb, rza, rxb, ga, gb, nn, squares,
    lsem, fs_sem, fr_sem, ms_sem, mr_sem, bs_sem, br_sem,
):
    z, x, c, y = (lax.axis_index(a) for a in ("z", "x", "c", "y"))
    pos = (z, x, c, y)

    local = []

    def load(src, dst):
        k = pltpu.make_async_copy(src, dst, lsem.at[len(local)])
        k.start()
        local.append(k)
        return k

    fl = [
        load(factors.at[:, pl.ds(16 * h, 16), :], fw.at[:, z, x, c, h]) for h in range(2)
    ]
    ml = load(master, own_f32)
    cl = load(cots, cin)
    xl = load(inputs, xin)
    el = [load(first, fm), load(second, sm)]

    barrier = pltpu.get_barrier_semaphore()
    peers = []
    for dz in range(1, NZ):
        peers.append((lax.rem(z + dz, NZ), x, c, y))
    for dx in range(1, NX):
        peers.append((z, lax.rem(x + dx, NX), c, y))
    for dy in range(1, 4):
        peers.append((z, x, c, lax.rem(y + dy, 4)))
    peers.append((z, x, 1 - c, y))
    for peer in peers:
        pl.semaphore_signal(barrier, inc=1, device_id=peer, device_id_type=MESH)
    ml.wait()
    for m in range(3):
        for h in range(2):
            mw[m, z, x, c, h] = coded(own_f32[m, 16 * h:16 * h + 16, :])
    for k in fl:
        k.wait()
    pl.semaphore_wait(barrier, len(peers))

    def turned(m):
        ct[pl.ds(256 * m, 256), :] = cin[m].T

    def gradient(lo, hi):
        def body(zz, _):
            at = pl.ds(pl.multiple_of(zz * 256, 256), 256)
            g_hi, g_lo = split(dot(ct[...], xin[:, at]))
            for m in range(3):
                gt[m, 0:256, at] = g_hi[256 * m:256 * (m + 1)]
                gt[m, 256:512, at] = g_lo[256 * m:256 * (m + 1)]
            return 0
        lax.fori_loop(lo, hi, body, 0)

    f = Gather(pos, fw, fs_sem, fr_sem, -1)
    w = Gather(pos, mw, ms_sem, mr_sem, 1)
    f.start()
    w.start()
    cl.wait()
    for m in range(3):
        turned(m)
    xl.wait()
    gradient(0, 3)
    f.near()
    f.far(1)
    f.cross(0)
    w.near()
    gradient(3, 5)
    for m in ORDER:
        f.ring(1, m)
    f.far(2)
    f.cross(1)
    f.cross2(0)
    w.far(1)
    w.cross(0)
    gradient(5, 7)
    for m in ORDER:
        f.ring(2, m)
    for m in ORDER:
        w.ring(1, m)
    f.far(3)
    f.cross(2)
    f.cross2(1)
    w.far(2)
    w.cross(1)
    w.cross2(0)
    gradient(7, 8)
    for m in ORDER:
        f.ring(3, m)
    f.far(4)
    f.cross(3)
    f.cross2(2)
    for m in ORDER:
        w.ring(2, m)
    f.cross(4)
    f.cross2(3)
    w.far(3)
    w.cross(2)
    w.cross2(1)
    f.cross2(4)
    f.ring(4, 2)
    f.ring(4, 0)
    f.ring(4, 1)

    started = []

    def send(src, dst, target):
        k = len(started)
        copy = pltpu.make_async_remote_copy(
            src_ref=src, dst_ref=dst, send_sem=bs_sem.at[k], recv_sem=br_sem.at[k], device_id=target, device_id_type=MESH
        )
        copy.start()
        started.append(copy)
        return copy

    def got(copies):
        for k in copies:
            k.wait_recv()

    partner = (z, x, 1 - c, y)

    def zpeer(dz):
        return lax.rem(z + (dz + NZ), NZ)

    def xpeer(dx):
        return lax.rem(x + (dx + NX), NX)

    zorder = (4, 3, -3, 2, -2, 1, -1)
    xorder = (2, 1, -1)

    def project(m):
        both = dot(gt[m], fw[m].reshape(D, 256))
        part = (both[:256] + both[256:]).T
        for half in range(2):
            cols = part[:, half * 128:(half + 1) * 128]
            if m < 2:
                for xx in range(NX):
                    pa[half, xx, m] = cols[xx * 64:(xx + 1) * 64]
            else:
                for zz in range(NZ):
                    pb[half, zz] = cols[zz * 32:(zz + 1) * 32]

    f.paired(2)
    project(2)
    k1 = send(pb.at[1 - c], cb, partner)
    f.paired(0)
    project(0)
    f.paired(1)
    project(1)
    k2 = send(pa.at[1 - c], ca, partner)
    for m in ORDER:
        w.ring(3, m)
    got([k1])
    sb[...] = pb[c] + cb[...]
    b1 = [send(sb.at[zpeer(dz)], rzb.at[i], (zpeer(dz), x, c, y)) for i, dz in enumerate(zorder)]
    got([k2])
    sa[...] = pa[c] + ca[...]
    a1 = [send(sa.at[xpeer(dx)], rxa.at[i], (z, xpeer(dx), c, y)) for i, dx in enumerate(xorder)]
    w.far(4)
    w.cross(3)
    w.cross2(2)
    got(a1)
    for m in range(2):
        tot = sa[x, m]
        for i in range(3):
            tot = tot + rxa[i, m]
        for zz in range(NZ):
            ta[zz, m] = tot[zz * 8:(zz + 1) * 8]
    a2 = [send(ta.at[zpeer(dz)], rza.at[i], (zpeer(dz), x, c, y)) for i, dz in enumerate(zorder)]
    w.cross(4)
    w.cross2(3)
    got(b1)
    tot = sb[z]
    for i in range(7):
        tot = tot + rzb[i]
    for xx in range(NX):
        tb[xx] = tot[xx * 8:(xx + 1) * 8]
    b2 = [send(tb.at[xpeer(dx)], rxb.at[i], (z, xpeer(dx), c, y)) for i, dx in enumerate(xorder)]
    w.cross2(4)
    for m in ORDER:
        w.ring(4, m)
    got(b2)
    tot = tb[x]
    for i in range(3):
        tot = tot + rxb[i]
    gb[c, z, x] = tot
    b3 = [send(gb.at[c, z, x], gb.at[c, z, x], (z, xpeer(dx), c, y)) for dx in xorder]
    got(a2)
    tot = ta[z]
    for i in range(7):
        tot = tot + rza[i]
    ga[c, x, z] = tot
    a3 = [send(ga.at[c, x, z], ga.at[c, x, z], (zpeer(dz), x, c, y)) for dz in zorder]

    def widen(m):
        def body(zz, _):
            wide[m, pl.ds(pl.multiple_of(zz * 256, 256), 256), :] = decoded(mw[m, zz].reshape(256, 256))
            return 0
        lax.fori_loop(0, NZ, body, 0)

    w.paired(2)
    widen(2)
    got(b3)
    b4 = [send(gb.at[c, z], gb.at[c, z], (zpeer(dz), x, c, y)) for dz in zorder]
    w.paired(0)
    widen(0)
    got(a3)
    a4 = [send(ga.at[c, x], ga.at[c, x], (z, xpeer(dx), c, y)) for dx in xorder]
    ka = [send(ga.at[c, x], ga.at[c, x], partner)]
    w.paired(1)
    widen(1)
    got(b4)
    kb = send(gb.at[c], gb.at[c], partner)
    for k in el:
        k.wait()
    got([kb])

    def moments(m):
        for half in range(2):
            cols = slice(half * 128, (half + 1) * 128)
            if m < 2:
                proj = jnp.concatenate([ga[half, xx, zz, m] for xx in range(NX) for zz in range(NZ)], axis=0)
            else:
                proj = jnp.concatenate([gb[half, zz, xx] for zz in range(NZ) for xx in range(NX)], axis=0)
            nf = beta_first * fm[m, :, cols] + (1.0 - beta_first) * proj
            ns = beta_second * sm[m, :, cols] + (1.0 - beta_second) * proj * proj
            fm[m, :, cols] = nf
            sm[m, :, cols] = ns
            hi, lo = split(nf / (jnp.sqrt(ns) + adam_eps))
            nn[m, 0:256, cols] = hi
            nn[m, 256:512, cols] = lo

    ys = {}

    def update(m):
        def body(zz, acc):
            fz = fw[m, pl.ds(2 * zz, 2)].reshape(512, 256)
            u = dot(jnp.concatenate([fz, fz], axis=1), nn[m])
            um[m, pl.ds(pl.multiple_of(zz * 512, 512), 512), :] = u
            uu = jnp.sum((u * u).reshape(64, 8, 256), axis=0)
            return acc + uu[:, :128] + uu[:, 128:]
        squares[y, m] = lax.fori_loop(0, 4, body, jnp.zeros((8, 128), F32))
        ys[m] = [send(squares.at[y, m], squares.at[y, m], (z, x, c, lax.rem(y + dy, 4))) for dy in (1, 2, 3)]

    moments(2)
    update(2)
    for i, dx in enumerate(xorder):
        got([a4[i]])
        ka.append(send(ga.at[c, xpeer(-dx)], ga.at[c, xpeer(-dx)], partner))
    got(ka)
    for m in (0, 1):
        moments(m)
        update(m)

    rows = pl.multiple_of(z * 256 + x * 64 + c * 32, 32)
    for m in ORDER:
        got(ys[m])
        tot = squares[0, m]
        for j in range(1, 4):
            tot = tot + squares[j, m]
        inv = 1.0 / jnp.sqrt(jnp.sum(tot, keepdims=True) / (D * MW) + norm_eps)
        step = um[m, pl.ds(rows, 32), :] * inv
        own_step[m] = step
        own_new[m] = own_f32[m] - learning_rate * step

        def body(zz, _):
            at = pl.ds(pl.multiple_of(zz * 256, 256), 256)
            copy_v[m, at, :] = (wide[m, at, :] - learning_rate * (um[m, at, :] * inv)).astype(BF)
            return 0
        lax.fori_loop(0, NZ, body, 0)
    f.drain()
    w.drain()
    for k in started:
        k.wait_send()


def write_out(*refs):
    sem = refs[-1]
    copies = [pltpu.make_async_copy(refs[i], refs[5 + i], sem.at[i]) for i in range(5)]
    for k in copies:
        k.start()
    for k in copies:
        k.wait()


def local(inputs, cotangents, factors, first_moment, second_moment, master):
    cots = jnp.transpose(cotangents, (1, 0, 2))
    hbm = pl.BlockSpec(memory_space=pltpu.HBM)
    V = pltpu.VMEM
    dma = pltpu.SemaphoreType.DMA
    results = pl.pallas_call(
        kernel,
        out_shape=(
            V((3, 32, 256), F32), V((3, 32, 256), F32), V((3, D, 256), BF), V((3, 256, 256), F32), V((3, 256, 256), F32),
        ),
        in_specs=[hbm] * 6,
        out_specs=(pl.BlockSpec(memory_space=pltpu.VMEM),) * 5,
        scratch_shapes=[
            V((1024, 2048), BF), V((3, 1024, 256), BF), V((768, 1024), BF),
            V((3, NZ, NX, 2, 2, 16, 256), BF), V((3, NZ, NX, 2, 2, 16, 256), BF), V((3, D, 256), F32),
            V((3, 512, D), BF), V((3, D, 256), F32), V((3, 32, 256), F32),
            V((2, NX, 2, 64, 128), F32), V((2, NZ, 32, 128), F32),
            V((NX, 2, 64, 128), F32), V((NZ, 32, 128), F32),
            V((NX, 2, 64, 128), F32), V((NZ, 32, 128), F32),
            V((3, 2, 64, 128), F32), V((7, 32, 128), F32),
            V((NZ, 2, 8, 128), F32), V((NX, 8, 128), F32),
            V((7, 2, 8, 128), F32), V((3, 8, 128), F32),
            V((2, NX, NZ, 2, 8, 128), F32), V((2, NZ, NX, 8, 128), F32),
            V((3, 512, 256), BF), V((4, 3, 8, 128), F32),
            dma((16,)),
            dma((GATHER_COPIES,)), dma((GATHER_COPIES,)), dma((GATHER_COPIES,)), dma((GATHER_COPIES,)),
            dma((64,)), dma((64,)),
        ],
        compiler_params=pltpu.CompilerParams(collective_id=0, has_side_effects=True, vmem_limit_bytes=58 * 1024 * 1024),
        name="update",
    )(inputs, cots, factors, first_moment, second_moment, master)
    return pl.pallas_call(
        write_out,
        out_shape=tuple(jax.ShapeDtypeStruct(r.shape, r.dtype) for r in results),
        in_specs=[pl.BlockSpec(memory_space=pl.ANY)] * 5,
        out_specs=(hbm,) * 5,
        scratch_shapes=[dma((5,))],
        compiler_params=pltpu.CompilerParams(vmem_limit_bytes=1024 * 1024),
        name="write_out",
    )(*results)


def solution(mesh):
    torus = Mesh(mesh.devices.reshape(NZ, NX, 2, mesh.shape["tp"]), ("z", "x", "c", "y"))
    fs = ("z", "x", "c")
    return jax.shard_map(
        local,
        mesh=torus,
        in_specs=(
            P(fs, None),
            P(fs, None, "y"),
            P(None, fs, None),
            P(None, None, "y"),
            P(None, None, "y"),
            P(None, fs, "y"),
        ),
        out_specs=(
            P(None, fs, "y"),
            P(None, fs, "y"),
            P(None, None, "y"),
            P(None, None, "y"),
            P(None, None, "y"),
        ),
        check_vma=False,
    )
```

time: 96.6 us -> 76.7 us (0.79)
  Pallas kernels: 86.5 us -> 76 us
  local copies, waits for them, and re-layouts: 8.72 us -> 0 us
    pallas_call x1 -> x2, Pallas kernels: 86.5 us -> 76 us  [the longest x1 73.7 us: local(): pl.pallas_call(kernel, out_shape=(V((3, 32, 256), F32), V((3, 32, 256), F...]
    unnamed x9 -> x0, local copies, waits for them, and re-layouts: 8.72 us -> none
where the time goes in v2:
time: 76.7 us; the launch traced here: 76.6 us
  Pallas kernels  76 us (99%)
    pallas_call x1, Pallas kernels, local(): pl.pallas_call(kernel, out_shape=(V((3, 32, 256), F32), V((3, 32, 256), F...  73.7 us
    pallas_call x1, Pallas kernels, local(): pl.pallas_call(write_out, out_shape=tuple((jax.ShapeDtypeStruct(r.shape,...  2.29 us

profile of v2, /device:TPU:1, one launch (start us, length us, event | category | flops | bytes accessed | tf_op | source)
XLA Modules:
  0.0 76.6 jit_solution(16861168839798436505)
XLA Ops:
  0.6 73.7 %update.1 = (f32[3,32,256]{2,1,0:T(8,128)S(1)}, f32[3,32,256]{2,1,0:T(8,128)S(1)}, bf16[3,2048,256]{2,1,0:T(8,128)(2,1)S(1)}, f32[3,256,256]{2,1,0:T(8,128)S(1)}, f32[3,256,256]{2,1,0:T(8,128)S(1)}) custom-call(bf16[1024,2048]{1,0:T(8,128)(2,1)} %inputs.1, bf16[3,1024,256]{2,1,0:T(8,128)(2,1)} %bitcast.1, bf16[3,32,256]{2,1,0:T(8,128)(2,1)} %factors.1, ...), custom_call_target="tpu_custom_call" | custom-call | tf_op jit(solution)/shard_map/update/pallas_call | solution.py:451
  74.3 2.3 %write_out.1 = (f32[3,32,256]{2,1,0:T(8,128)}, f32[3,32,256]{2,1,0:T(8,128)}, bf16[3,2048,256]{2,1,0:T(8,128)(2,1)}, f32[3,256,256]{2,1,0:T(8,128)}, f32[3,256,256]{2,1,0:T(8,128)}) custom-call(f32[3,32,256]{2,1,0:T(8,128)S(1)} %get-tuple-element.10.refs_0_, f32[3,32,256]{2,1,0:T(8,128)S(1)} %get-tuple-element.11.refs_1_, ...), custom_call_target="tpu_custom_call" | custom-call | tf_op jit(solution)/shard_map/write_out/pallas_call | solution.py:477

commit v3 on v2

v3 whole, which is shorter than its diff:
```python
import math

import jax
import jax.numpy as jnp
from jax import lax
from jax.experimental import pallas as pl
from jax.experimental.pallas import tpu as pltpu
from jax.sharding import Mesh
from jax.sharding import PartitionSpec as P

D = 2048
MW = 1024
BF = jnp.bfloat16
F32 = jnp.float32
MESH = pl.DeviceIdType.MESH

beta_first = 0.8
beta_second = 0.9
adam_eps = 1e-08
norm_eps = 1e-06
learning_rate = 0.005

NZ, NX = 8, 4
GROUPS = 40
ORDER = (0, 1, 2)


class Copies:
    def __init__(self, pos, ssem, rsem, room):
        self.z, self.x, self.c, self.y = pos
        self.ssem, self.rsem, self.room = ssem, rsem, room
        self.sent = 0
        self.groups = {}

    def zof(self, dz):
        return lax.rem(self.z + (dz + NZ), NZ)

    def xof(self, dx):
        return lax.rem(self.x + (dx + NX), NX)

    def send(self, key, src, dst=None, dz=0, dx=0, dy=0, other=False):
        dst = src if dst is None else dst
        if key not in self.groups:
            self.groups[key] = [len(self.groups), 0]
        group = self.groups[key]
        size = math.prod(src.shape) * jnp.dtype(src.dtype).itemsize
        group[1] += size
        self.sent += size
        pltpu.make_async_remote_copy(
            src_ref=src, dst_ref=dst, send_sem=self.ssem.at[0], recv_sem=self.rsem.at[group[0]],
            device_id=(self.zof(dz), self.xof(dx), 1 - self.c if other else self.c, lax.rem(self.y + dy, 4)), device_id_type=MESH,
        ).start()

    def bytes_at(self, sem, size):
        part = self.room.at[pl.ds(0, size // 4096)]
        pltpu.make_async_copy(part, part, sem).wait()

    def got(self, key):
        self.bytes_at(self.rsem.at[self.groups[key][0]], self.groups[key][1])

    def drain(self):
        self.bytes_at(self.ssem.at[0], self.sent)


class Gather(Copies):
    def __init__(self, pos, whole, ssem, rsem, room, flip, rows):
        super().__init__(pos, ssem, rsem, room)
        self.b = whole
        self.flip = flip
        self.q0, self.q1 = pl.ds(0, rows // 8), pl.ds(rows // 8, 4 - rows // 8)

    def blk(self, dz, m, part=None):
        xs = slice(None) if part is None else pl.ds(2 * part, 2)
        return self.b.at[m, self.zof(dz), xs, self.c, self.q0]

    def one(self, dz, dx):
        return self.b.at[:, self.zof(dz), self.xof(dx), self.c, self.q1]

    def line(self, dz):
        return self.b.at[:, self.zof(dz), :, self.c, self.q1]

    def start_x(self):
        own = self.b.at[:, self.z, self.x, self.c, self.q0]
        for dx in (2, 1, -1):
            self.send("near", own, dx=dx)

    def cross_start(self, k, offsets):
        for dz in offsets:
            for dx in (1, -1):
                self.send(("cross", k), self.one(dz, 0), dx=dx)

    def cross_on(self, k, offsets):
        self.got(("cross", k))
        for dz in offsets:
            side = self.flip if dz % 2 else -self.flip
            self.send(("cross2", k), self.one(dz, side), dx=-side)

    def cross_end(self, k, offsets, key):
        self.got(("cross2", k))
        for dz in offsets:
            self.send(key, self.line(dz), other=True)


NEAR_Z, FAR_Z = (1, -1, 2, -2), (3, -3, 4)


class Direct(Gather):
    def own0(self):
        return self.b.at[pl.ds(0, 2), self.z, :, self.c, self.q0]

    def one(self, dz, dx):
        return self.b.at[pl.ds(0, 2), self.zof(dz), self.xof(dx), self.c, self.q1]

    def line(self, dz):
        return self.b.at[pl.ds(0, 2), self.zof(dz), :, self.c, self.q1]

    def column(self, dx):
        return self.b.at[2, :, self.xof(dx), self.c, self.y]

    def start(self):
        own = self.b.at[pl.ds(0, 2), self.z, self.x, self.c, self.q0]
        for dx in (2, 1, -1):
            self.send("near", own, dx=dx)
        own = self.b.at[2, self.z, self.x, self.c, self.y]
        for dz in FAR_Z + NEAR_Z:
            self.send("quarter", own, dz=dz)
        for dz in NEAR_Z:
            self.send(("far", 1), self.one(0, 0), dz=dz)
        self.line_start(0, (0,))
        for dz in FAR_Z:
            self.send(("far", 2), self.one(0, 0), dz=dz)

    def line_start(self, k, offsets):
        for dz in offsets:
            for dx in (2, 1, -1):
                self.send(("cross", k), self.one(dz, 0), dx=dx)

    def near(self):
        self.got("near")
        for k, offsets in ((1, NEAR_Z), (2, FAR_Z)):
            for dz in offsets:
                self.send(("ring", k), self.own0(), dz=dz)
        self.send("early", self.own0(), other=True)

    def quarter(self):
        self.got("quarter")
        for dx in (2, 1, -1):
            self.send("columns", self.column(0), dx=dx)
        for dy in (2, 1, 3):
            self.send("exchange", self.column(0), dy=dy)

    def columns(self):
        self.got("columns")
        for dx in (1, -1, 2):
            for dy in (2, 1, 3):
                self.send("exchange", self.column(dx), dy=dy)
        self.send("last", self.b.at[2, :, :, self.c, self.y], other=True)

    def exchange(self):
        self.got("exchange")
        for dy in (1, 2, 3):
            self.send("last", self.b.at[2, :, :, self.c, lax.rem(self.y + dy, 4)], other=True)

    def ring(self, k, offsets, key):
        self.got(("ring", k))
        for dz in offsets:
            self.send(key, self.b.at[pl.ds(0, 2), self.zof(dz), :, self.c, self.q0], other=True)

    def far(self, k, offsets):
        self.got(("far", k))
        self.line_start(k, offsets)

    def line_end(self, k, offsets, key):
        self.got(("cross", k))
        for dz in offsets:
            self.send(key, self.line(dz), other=True)


class Ring(Gather):
    def both(self, k):
        return (k, -k) if 0 < k < 4 else (self.flip * k,)

    def start(self):
        self.start_x()
        for dz in (1, -1):
            self.send(("far", 1), self.one(0, 0), dz=dz)
        self.cross_start(0, (0,))

    def near(self):
        self.got("near")
        for m in ORDER:
            for dz in (1, -1):
                self.send(("ring", 1, m), self.blk(0, m), dz=dz)
        for m in ORDER:
            self.send("early", self.blk(0, m), other=True)

    def ring(self, k, m):
        self.got(("ring", k, m))
        if k < 4:
            for side in (-1, 1):
                part = None if k < 3 else (0 if side < 0 else 1)
                self.send(("ring", k + 1, m), self.blk(side * k, m, part), dz=-side)
            for side in (-1, 1):
                self.send("early" if k < 3 else ("late", m), self.blk(side * k, m), other=True)
        else:
            self.send(("late", m), self.blk(4, m), other=True)

    def far(self, k):
        self.got(("far", k))
        for dz in self.both(k):
            if k < 3 or (k == 3 and dz * self.flip > 0):
                self.send(("far", k + 1), self.one(dz, 0), dz=1 if dz < 0 else -1)
        self.cross_start(k, self.both(k))

    def cross(self, k):
        self.cross_on(k, self.both(k))

    def cross2(self, k):
        self.cross_end(k, self.both(k), "early" if k < 3 else ("late", 0))


def split(value):
    high = value.astype(BF)
    return high, (value - high.astype(F32)).astype(BF)


FLOOR = 2.0 ** -124


def coded(value):
    t = jnp.abs(value) * 8.0
    t = t * t
    t = t * t
    t = t * t * 2.0 ** 60
    t = jnp.maximum(t * t, FLOOR)
    return jnp.where(value < 0, -t, t).astype(BF)


def decoded(code):
    t = code.astype(F32)
    size = jnp.abs(t)
    root = jnp.exp(jnp.log(size) / 16.0) * (2.0 ** -7.5 / 8.0)
    root = jnp.where(size > FLOOR, root, 0.0)
    return jnp.where(t < 0, -root, root)


def dot(a, b):
    return lax.dot_general(a, b, (((1,), (0,)), ((), ())), preferred_element_type=F32)


def kernel(
    inputs, cots, factors, first, second, master,
    own_step, own_new, copy_v, fm, sm,
    xin, cin, ct, fw, mw, wide, gt, both_v, um, own_f32,
    pa, pb, ca, cb, sa, sb, rxa, rzb, ta, tb, rza, rxb, ga, gb, nn, squares, room,
    lsem, fs_sem, fr_sem, ms_sem, mr_sem, bs_sem, br_sem,
):
    z, x, c, y = (lax.axis_index(a) for a in ("z", "x", "c", "y"))
    pos = (z, x, c, y)

    local = []

    def load(src, dst):
        k = pltpu.make_async_copy(src, dst, lsem.at[len(local)])
        k.start()
        local.append(k)
        return k

    fl = [load(factors.at[pl.ds(0, 2), pl.ds(8 * q, 8), :], fw.at[pl.ds(0, 2), z, x, c, q]) for q in range(4)]
    fl.append(load(factors.at[2, pl.ds(pl.multiple_of(8 * y, 8), 8), :], fw.at[2, z, x, c, y]))
    ml = load(master, own_f32)
    cl = load(cots, cin)
    xl = load(inputs, xin)
    el = [load(first, fm), load(second, sm)]

    barrier = pltpu.get_barrier_semaphore()
    peers = []
    for dz in range(1, NZ):
        peers.append((lax.rem(z + dz, NZ), x, c, y))
    for dx in range(1, NX):
        peers.append((z, lax.rem(x + dx, NX), c, y))
    for dy in range(1, 4):
        peers.append((z, x, c, lax.rem(y + dy, 4)))
    peers.append((z, x, 1 - c, y))
    for peer in peers:
        pl.semaphore_signal(barrier, inc=1, device_id=peer, device_id_type=MESH)
    ml.wait()
    for m in range(3):
        mw[m, z, x, c] = coded(own_f32[m]).reshape(4, 8, 256)
    for k in fl:
        k.wait()
    pl.semaphore_wait(barrier, len(peers))

    def turned(m):
        ct[pl.ds(256 * m, 256), :] = cin[m].T

    def gradient(lo, hi):
        def body(zz, _):
            at = pl.ds(pl.multiple_of(zz * 256, 256), 256)
            g_hi, g_lo = split(dot(ct[...], xin[:, at]))
            for m in range(3):
                gt[m, zz, 0:256] = g_hi[256 * m:256 * (m + 1)]
                gt[m, zz, 256:512] = g_lo[256 * m:256 * (m + 1)]
            return 0
        lax.fori_loop(lo, hi, body, 0)

    f = Direct(pos, fw, fs_sem, fr_sem, room, -1, 8)
    w = Ring(pos, mw, ms_sem, mr_sem, room, 1, 16)
    r = Copies(pos, bs_sem, br_sem, room)

    def product(m, offsets):
        zs = [f.zof(dz) for dz in offsets]
        return dot(
            jnp.concatenate([gt[m, zz] for zz in zs], axis=1),
            jnp.concatenate([fw[m, zz].reshape(256, 256) for zz in zs], axis=0),
        )

    def project(m):
        if m == 2:
            both = product(m, range(8))
        else:
            both = both_v[m] + product(m, FAR_Z)
        part = (both[:256] + both[256:]).T
        for half in range(2):
            cols = part[:, half * 128:(half + 1) * 128]
            if m < 2:
                for xx in range(NX):
                    pa[half, m, xx] = cols[xx * 64:(xx + 1) * 64]
            else:
                for zz in range(NZ):
                    pb[half, zz] = cols[zz * 32:(zz + 1) * 32]

    zorder = (4, 3, -3, 2, -2, 1, -1)
    xorder = (2, 1, -1)

    def widen(m):
        def body(zz, _):
            at = pl.ds(pl.multiple_of(m * D + zz * 256, 256), 256)
            wide[at, :] = decoded(mw[m, zz].reshape(256, 256))
            return 0
        lax.fori_loop(0, NZ, body, 0)

    def moments(m):
        for half in range(2):
            cols = slice(half * 128, (half + 1) * 128)
            if m < 2:
                proj = jnp.concatenate([ga[half, m, xx, zz] for xx in range(NX) for zz in range(NZ)], axis=0)
            else:
                proj = jnp.concatenate([gb[half, zz, xx] for zz in range(NZ) for xx in range(NX)], axis=0)
            nf = beta_first * fm[m, :, cols] + (1.0 - beta_first) * proj
            ns = beta_second * sm[m, :, cols] + (1.0 - beta_second) * proj * proj
            fm[m, :, cols] = nf
            sm[m, :, cols] = ns
            hi, lo = split(nf / (jnp.sqrt(ns) + adam_eps))
            nn[m, 0:256, cols] = hi
            nn[m, 256:512, cols] = lo

    def update(m):
        def body(zz, acc):
            fz = fw[m, pl.ds(4 * zz, 4)].reshape(1024, 256)
            u = dot(jnp.concatenate([fz, fz], axis=1), nn[m])
            um[m, pl.ds(pl.multiple_of(zz * 1024, 1024), 1024), :] = u
            uu = jnp.sum((u * u).reshape(128, 8, 256), axis=0)
            return acc + uu[:, :128] + uu[:, 128:]
        squares[y, m] = lax.fori_loop(0, 2, body, jnp.zeros((8, 128), F32))
        for dy in (1, 2, 3):
            r.send(("ys", m), squares.at[y, m], dy=dy)

    f.start()
    cl.wait()
    for m in range(3):
        turned(m)
    xl.wait()
    gradient(0, 2)
    f.quarter()
    f.near()
    f.far(1, NEAR_Z)
    gradient(2, 4)
    f.line_end(0, (0,), "early")
    f.far(2, FAR_Z)
    gradient(4, 6)
    f.columns()
    gradient(6, 8)
    f.ring(1, NEAR_Z, "early")
    w.start()
    f.line_end(1, NEAR_Z, "early")
    f.ring(2, FAR_Z, "late")
    f.line_end(2, FAR_Z, "late")
    f.got("early")
    for m in range(2):
        both_v[m] = product(m, (0,) + NEAR_Z)
    f.exchange()
    w.far(1)
    w.cross(0)
    w.near()
    f.got("late")
    for m in range(2):
        project(m)
        r.send(("k", m), pa.at[1 - c, m], ca.at[m], other=True)
    f.got("last")
    project(2)
    r.send(("k", 2), pb.at[1 - c], cb, other=True)
    for m in range(2):
        r.got(("k", m))
        sa[m] = pa[c, m] + ca[m]
        for i, dx in enumerate(xorder):
            r.send(("a1", m), sa.at[m, r.xof(dx)], rxa.at[m, i], dx=dx)
    r.got(("k", 2))
    sb[...] = pb[c] + cb[...]
    for i, dz in enumerate(zorder):
        r.send("b1", sb.at[r.zof(dz)], rzb.at[i], dz=dz)
    w.far(2)
    w.cross(1)
    w.cross2(0)
    for m in ORDER:
        w.ring(1, m)
    for m in range(2):
        r.got(("a1", m))
        tot = sa[m, x]
        for i in range(3):
            tot = tot + rxa[m, i]
        for zz in range(NZ):
            ta[m, zz] = tot[zz * 8:(zz + 1) * 8]
        for i, dz in enumerate(zorder):
            r.send(("a2", m), ta.at[m, r.zof(dz)], rza.at[m, i], dz=dz)
    w.far(3)
    w.cross(2)
    w.cross2(1)
    r.got("b1")
    tot = sb[z]
    for i in range(7):
        tot = tot + rzb[i]
    for xx in range(NX):
        tb[xx] = tot[xx * 8:(xx + 1) * 8]
    for i, dx in enumerate(xorder):
        r.send("b2", tb.at[r.xof(dx)], rxb.at[i], dx=dx)
    for m in ORDER:
        w.ring(2, m)
    for m in range(2):
        r.got(("a2", m))
        tot = ta[m, z]
        for i in range(7):
            tot = tot + rza[m, i]
        ga[c, m, x, z] = tot
        for dz in zorder:
            r.send(("a3", m), ga.at[c, m, x, z], dz=dz)
    r.got("b2")
    tot = tb[x]
    for i in range(3):
        tot = tot + rxb[i]
    gb[c, z, x] = tot
    for dx in xorder:
        r.send("b3", gb.at[c, z, x], dx=dx)
    w.far(4)
    w.cross(3)
    w.cross2(2)
    for m in ORDER:
        w.ring(3, m)
    r.got("b3")
    for dz in zorder:
        r.send("b4", gb.at[c, z], dz=dz)
    for m in range(2):
        r.got(("a3", m))
        for dx in xorder:
            r.send(("a4", m), ga.at[c, m, x], dx=dx)
        r.send(("ka", m), ga.at[c, m, x], other=True)
    for k in el:
        k.wait()
    w.cross(4)
    w.cross2(3)
    for m in ORDER:
        w.ring(4, m)
    for m in range(2):
        r.got(("a4", m))
        for dx in xorder:
            r.send(("ka", m), ga.at[c, m, r.xof(-dx)], other=True)
    r.got("b4")
    r.send("kb", gb.at[c], other=True)
    w.cross2(4)
    for m in range(2):
        r.got(("ka", m))
        moments(m)
        update(m)
    r.got("kb")
    moments(2)
    update(2)
    w.got("early")
    for m in ORDER:
        w.got(("late", m))
        widen(m)

    rows = pl.multiple_of(z * 256 + x * 64 + c * 32, 32)
    for m in ORDER:
        r.got(("ys", m))
        tot = squares[0, m]
        for j in range(1, 4):
            tot = tot + squares[j, m]
        inv = 1.0 / jnp.sqrt(jnp.sum(tot, keepdims=True) / (D * MW) + norm_eps)
        step = um[m, pl.ds(rows, 32), :] * inv
        own_step[m] = step
        own_new[m] = own_f32[m] - learning_rate * step

        def body(zz, _):
            at = pl.ds(pl.multiple_of(zz * 256, 256), 256)
            copy_v[m, at, :] = (wide[pl.ds(pl.multiple_of(m * D + zz * 256, 256), 256), :] - learning_rate * (um[m, at, :] * inv)).astype(BF)
            return 0
        lax.fori_loop(0, NZ, body, 0)
    f.drain()
    w.drain()
    r.drain()


def write_out(*refs):
    sem = refs[-1]
    copies = []
    for i in (2, 3, 4, 0, 1):
        for m in range(3):
            copies.append(pltpu.make_async_copy(refs[i].at[m], refs[5 + i].at[m], sem.at[len(copies)]))
    for k in copies:
        k.start()
    for k in copies:
        k.wait()


def local(inputs, cotangents, factors, first_moment, second_moment, master):
    cots = jnp.transpose(cotangents, (1, 0, 2))
    hbm = pl.BlockSpec(memory_space=pltpu.HBM)
    V = pltpu.VMEM
    dma = pltpu.SemaphoreType.DMA
    results = pl.pallas_call(
        kernel,
        out_shape=(
            V((3, 32, 256), F32), V((3, 32, 256), F32), V((3, D, 256), BF), V((3, 256, 256), F32), V((3, 256, 256), F32),
        ),
        in_specs=[hbm] * 6,
        out_specs=(pl.BlockSpec(memory_space=pltpu.VMEM),) * 5,
        scratch_shapes=[
            V((1024, 2048), BF), V((3, 1024, 256), BF), V((768, 1024), BF),
            V((3, NZ, NX, 2, 4, 8, 256), BF), V((3, NZ, NX, 2, 4, 8, 256), BF), V((3 * D, 256), F32),
            V((3, NZ, 512, 256), BF), V((3, 512, 256), F32), V((3, D, 256), F32), V((3, 32, 256), F32),
            V((2, 2, NX, 64, 128), F32), V((2, NZ, 32, 128), F32),
            V((2, NX, 64, 128), F32), V((NZ, 32, 128), F32),
            V((2, NX, 64, 128), F32), V((NZ, 32, 128), F32),
            V((2, 3, 64, 128), F32), V((7, 32, 128), F32),
            V((2, NZ, 8, 128), F32), V((NX, 8, 128), F32),
            V((2, 7, 8, 128), F32), V((3, 8, 128), F32),
            V((2, 2, NX, NZ, 8, 128), F32), V((2, NZ, NX, 8, 128), F32),
            V((3, 512, 256), BF), V((4, 3, 8, 128), F32), V((1024, 8, 128), F32),
            dma((16,)),
            dma((1,)), dma((GROUPS,)), dma((1,)), dma((GROUPS,)),
            dma((1,)), dma((GROUPS,)),
        ],
        compiler_params=pltpu.CompilerParams(collective_id=0, has_side_effects=True, vmem_limit_bytes=58 * 1024 * 1024),
        name="update",
    )(inputs, cots, factors, first_moment, second_moment, master)
    return pl.pallas_call(
        write_out,
        out_shape=tuple(jax.ShapeDtypeStruct(r.shape, r.dtype) for r in results),
        in_specs=[pl.BlockSpec(memory_space=pl.ANY)] * 5,
        out_specs=(hbm,) * 5,
        scratch_shapes=[dma((15,))],
        compiler_params=pltpu.CompilerParams(vmem_limit_bytes=1024 * 1024),
        name="write_out",
    )(*results)


def solution(mesh):
    torus = Mesh(mesh.devices.reshape(NZ, NX, 2, mesh.shape["tp"]), ("z", "x", "c", "y"))
    fs = ("z", "x", "c")
    return jax.shard_map(
        local,
        mesh=torus,
        in_specs=(
            P(fs, None),
            P(fs, None, "y"),
            P(None, fs, None),
            P(None, None, "y"),
            P(None, None, "y"),
            P(None, fs, "y"),
        ),
        out_specs=(
            P(None, fs, "y"),
            P(None, fs, "y"),
            P(None, None, "y"),
            P(None, None, "y"),
            P(None, None, "y"),
        ),
        check_vma=False,
    )
```

time: 76.7 us -> 61.7 us (0.80)
  Pallas kernels: 76 us -> 60.9 us
    pallas_call x1, Pallas kernels: 73.7 us -> 58.6 us  [local(): pl.pallas_call(kernel, out_shape=(V((3, 32, 256), F32), V((3, 32, 256), F...]
where the time goes in v3:
time: 61.7 us; the launch traced here: 61.6 us
  Pallas kernels  60.9 us (99%)
  between operations  0.64 us (1%)
    pallas_call x1, Pallas kernels, local(): pl.pallas_call(kernel, out_shape=(V((3, 32, 256), F32), V((3, 32, 256), F...  58.6 us
    pallas_call x1, Pallas kernels, local(): pl.pallas_call(write_out, out_shape=tuple((jax.ShapeDtypeStruct(r.shape,...  2.33 us

profile of v3, /device:TPU:1, one launch (start us, length us, event | category | flops | bytes accessed | tf_op | source)
XLA Modules:
  0.0 61.6 jit_solution(14635343125266572415)
XLA Ops:
  0.6 58.6 %update.1 = (f32[3,32,256]{2,1,0:T(8,128)S(1)}, f32[3,32,256]{2,1,0:T(8,128)S(1)}, bf16[3,2048,256]{2,1,0:T(8,128)(2,1)S(1)}, f32[3,256,256]{2,1,0:T(8,128)S(1)}, f32[3,256,256]{2,1,0:T(8,128)S(1)}) custom-call(bf16[1024,2048]{1,0:T(8,128)(2,1)} %inputs.1, bf16[3,1024,256]{2,1,0:T(8,128)(2,1)} %bitcast.1, bf16[3,32,256]{2,1,0:T(8,128)(2,1)} %factors.1, ...), custom_call_target="tpu_custom_call" | custom-call | tf_op jit(solution)/shard_map/update/pallas_call | solution.py:530
  59.2 2.3 %write_out.1 = (f32[3,32,256]{2,1,0:T(8,128)}, f32[3,32,256]{2,1,0:T(8,128)}, bf16[3,2048,256]{2,1,0:T(8,128)(2,1)}, f32[3,256,256]{2,1,0:T(8,128)}, f32[3,256,256]{2,1,0:T(8,128)}) custom-call(f32[3,32,256]{2,1,0:T(8,128)S(1)} %get-tuple-element.10.refs_0_, f32[3,32,256]{2,1,0:T(8,128)S(1)} %get-tuple-element.11.refs_1_, ...), custom_call_target="tpu_custom_call" | custom-call | tf_op jit(solution)/shard_map/write_out/pallas_call | solution.py:556

commit v4 on v3

--- a/solution.py
+++ b/solution.py
@@ -224,24 +224,19 @@
     return high, (value - high.astype(F32)).astype(BF)
 
 
-FLOOR = 2.0 ** -124
+CODE_SCALE, CODE_SHIFT = 250.0 / math.sqrt(0.125), 125.0
 
 
 def coded(value):
-    t = jnp.abs(value) * 8.0
-    t = t * t
-    t = t * t
-    t = t * t * 2.0 ** 60
-    t = jnp.maximum(t * t, FLOOR)
+    t = jnp.exp2(jnp.sqrt(jnp.abs(value)) * CODE_SCALE - CODE_SHIFT)
     return jnp.where(value < 0, -t, t).astype(BF)
 
 
 def decoded(code):
     t = code.astype(F32)
-    size = jnp.abs(t)
-    root = jnp.exp(jnp.log(size) / 16.0) * (2.0 ** -7.5 / 8.0)
-    root = jnp.where(size > FLOOR, root, 0.0)
-    return jnp.where(t < 0, -root, root)
+    root = jnp.log(jnp.abs(t)) * (1.0 / (math.log(2.0) * CODE_SCALE)) + CODE_SHIFT / CODE_SCALE
+    size = root * root
+    return jnp.where(t < 0, -size, size)
 
 
 def dot(a, b):
@@ -257,21 +252,6 @@
 ):
     z, x, c, y = (lax.axis_index(a) for a in ("z", "x", "c", "y"))
     pos = (z, x, c, y)
-
-    local = []
-
-    def load(src, dst):
-        k = pltpu.make_async_copy(src, dst, lsem.at[len(local)])
-        k.start()
-        local.append(k)
-        return k
-
-    fl = [load(factors.at[pl.ds(0, 2), pl.ds(8 * q, 8), :], fw.at[pl.ds(0, 2), z, x, c, q]) for q in range(4)]
-    fl.append(load(factors.at[2, pl.ds(pl.multiple_of(8 * y, 8), 8), :], fw.at[2, z, x, c, y]))
-    ml = load(master, own_f32)
-    cl = load(cots, cin)
-    xl = load(inputs, xin)
-    el = [load(first, fm), load(second, sm)]
 
     barrier = pltpu.get_barrier_semaphore()
     peers = []
@@ -284,6 +264,21 @@
     peers.append((z, x, 1 - c, y))
     for peer in peers:
         pl.semaphore_signal(barrier, inc=1, device_id=peer, device_id_type=MESH)
+    local = []
+
+    def load(src, dst):
+        k = pltpu.make_async_copy(src, dst, lsem.at[len(local)])
+        k.start()
+        local.append(k)
+        return k
+
+    fl = [load(factors.at[pl.ds(0, 2), pl.ds(8 * q, 8), :], fw.at[pl.ds(0, 2), z, x, c, q]) for q in range(4)]
+    fl.append(load(factors.at[2, pl.ds(pl.multiple_of(8 * y, 8), 8), :], fw.at[2, z, x, c, y]))
+    ml = load(master, own_f32)
+    cl = load(cots, cin)
+    xl = load(inputs, xin)
+    el = [load(first, fm), load(second, sm)]
+
     ml.wait()
     for m in range(3):
         mw[m, z, x, c] = coded(own_f32[m]).reshape(4, 8, 256)
@@ -305,7 +300,7 @@
         lax.fori_loop(lo, hi, body, 0)
 
     f = Direct(pos, fw, fs_sem, fr_sem, room, -1, 8)
-    w = Ring(pos, mw, ms_sem, mr_sem, room, 1, 16)
+    w = Ring(pos, mw, ms_sem, mr_sem, room, 1, 8)
     r = Copies(pos, bs_sem, br_sem, room)
 
     def product(m, offsets):
@@ -372,8 +367,8 @@
         turned(m)
     xl.wait()
     gradient(0, 2)
+    f.near()
     f.quarter()
-    f.near()
     f.far(1, NEAR_Z)
     gradient(2, 4)
     f.line_end(0, (0,), "early")
@@ -397,14 +392,18 @@
     for m in range(2):
         project(m)
         r.send(("k", m), pa.at[1 - c, m], ca.at[m], other=True)
-    f.got("last")
-    project(2)
-    r.send(("k", 2), pb.at[1 - c], cb, other=True)
-    for m in range(2):
+
+    def reduce_a1(m):
         r.got(("k", m))
         sa[m] = pa[c, m] + ca[m]
         for i, dx in enumerate(xorder):
             r.send(("a1", m), sa.at[m, r.xof(dx)], rxa.at[m, i], dx=dx)
+
+    f.got("last")
+    reduce_a1(0)
+    project(2)
+    r.send(("k", 2), pb.at[1 - c], cb, other=True)
+    reduce_a1(1)
     r.got(("k", 2))
     sb[...] = pb[c] + cb[...]
     for i, dz in enumerate(zorder):
@@ -412,8 +411,6 @@
     w.far(2)
     w.cross(1)
     w.cross2(0)
-    for m in ORDER:
-        w.ring(1, m)
     for m in range(2):
         r.got(("a1", m))
         tot = sa[m, x]
@@ -423,9 +420,6 @@
             ta[m, zz] = tot[zz * 8:(zz + 1) * 8]
         for i, dz in enumerate(zorder):
             r.send(("a2", m), ta.at[m, r.zof(dz)], rza.at[m, i], dz=dz)
-    w.far(3)
-    w.cross(2)
-    w.cross2(1)
     r.got("b1")
     tot = sb[z]
     for i in range(7):
@@ -435,7 +429,10 @@
     for i, dx in enumerate(xorder):
         r.send("b2", tb.at[r.xof(dx)], rxb.at[i], dx=dx)
     for m in ORDER:
-        w.ring(2, m)
+        w.ring(1, m)
+    w.far(3)
+    w.cross(2)
+    w.cross2(1)
     for m in range(2):
         r.got(("a2", m))
         tot = ta[m, z]
@@ -451,11 +448,11 @@
     gb[c, z, x] = tot
     for dx in xorder:
         r.send("b3", gb.at[c, z, x], dx=dx)
+    for m in ORDER:
+        w.ring(2, m)
     w.far(4)
     w.cross(3)
     w.cross2(2)
-    for m in ORDER:
-        w.ring(3, m)
     r.got("b3")
     for dz in zorder:
         r.send("b4", gb.at[c, z], dz=dz)
@@ -466,10 +463,10 @@
         r.send(("ka", m), ga.at[c, m, x], other=True)
     for k in el:
         k.wait()
+    for m in ORDER:
+        w.ring(3, m)
     w.cross(4)
     w.cross2(3)
-    for m in ORDER:
-        w.ring(4, m)
     for m in range(2):
         r.got(("a4", m))
         for dx in xorder:
@@ -477,6 +474,8 @@
     r.got("b4")
     r.send("kb", gb.at[c], other=True)
     w.cross2(4)
+    for m in ORDER:
+        w.ring(4, m)
     for m in range(2):
         r.got(("ka", m))
         moments(m)

time: 61.7 us -> 60 us (0.972)
  Pallas kernels: 60.9 us -> 59.3 us
    pallas_call x1, Pallas kernels: 58.6 us -> 57 us  [local(): pl.pallas_call(kernel, out_shape=(V((3, 32, 256), F32), V((3, 32, 256), F...]
where the time goes in v4:
time: 60 us; the launch traced here: 59.9 us
  Pallas kernels  59.3 us (99%)
  between operations  0.64 us (1%)
    pallas_call x1, Pallas kernels, local(): pl.pallas_call(kernel, out_shape=(V((3, 32, 256), F32), V((3, 32, 256), F...  57 us
    pallas_call x1, Pallas kernels, local(): pl.pallas_call(write_out, out_shape=tuple((jax.ShapeDtypeStruct(r.shape,...  2.33 us

profile of v4, /device:TPU:1, one launch (start us, length us, event | category | flops | bytes accessed | tf_op | source)
XLA Modules:
  0.0 59.9 jit_solution(13855158951890659678)
XLA Ops:
  0.6 57.0 %update.1 = (f32[3,32,256]{2,1,0:T(8,128)S(1)}, f32[3,32,256]{2,1,0:T(8,128)S(1)}, bf16[3,2048,256]{2,1,0:T(8,128)(2,1)S(1)}, f32[3,256,256]{2,1,0:T(8,128)S(1)}, f32[3,256,256]{2,1,0:T(8,128)S(1)}) custom-call(bf16[1024,2048]{1,0:T(8,128)(2,1)} %inputs.1, bf16[3,1024,256]{2,1,0:T(8,128)(2,1)} %bitcast.1, bf16[3,32,256]{2,1,0:T(8,128)(2,1)} %factors.1, ...), custom_call_target="tpu_custom_call" | custom-call | tf_op jit(solution)/shard_map/update/pallas_call | solution.py:529
  57.6 2.3 %write_out.1 = (f32[3,32,256]{2,1,0:T(8,128)}, f32[3,32,256]{2,1,0:T(8,128)}, bf16[3,2048,256]{2,1,0:T(8,128)(2,1)}, f32[3,256,256]{2,1,0:T(8,128)}, f32[3,256,256]{2,1,0:T(8,128)}) custom-call(f32[3,32,256]{2,1,0:T(8,128)S(1)} %get-tuple-element.10.refs_0_, f32[3,32,256]{2,1,0:T(8,128)S(1)} %get-tuple-element.11.refs_1_, ...), custom_call_target="tpu_custom_call" | custom-call | tf_op jit(solution)/shard_map/write_out/pallas_call | solution.py:555

commit v5 on v4

--- a/solution.py
+++ b/solution.py
@@ -246,7 +246,7 @@
 def kernel(
     inputs, cots, factors, first, second, master,
     own_step, own_new, copy_v, fm, sm,
-    xin, cin, ct, fw, mw, wide, gt, both_v, um, own_f32,
+    xin, cin, ct, fw, mw, wide, gt, um, own_f32,
     pa, pb, ca, cb, sa, sb, rxa, rzb, ta, tb, rza, rxb, ga, gb, nn, squares, room,
     lsem, fs_sem, fr_sem, ms_sem, mr_sem, bs_sem, br_sem,
 ):
@@ -303,18 +303,11 @@
     w = Ring(pos, mw, ms_sem, mr_sem, room, 1, 8)
     r = Copies(pos, bs_sem, br_sem, room)
 
-    def product(m, offsets):
-        zs = [f.zof(dz) for dz in offsets]
-        return dot(
-            jnp.concatenate([gt[m, zz] for zz in zs], axis=1),
-            jnp.concatenate([fw[m, zz].reshape(256, 256) for zz in zs], axis=0),
+    def project(m):
+        both = dot(
+            jnp.concatenate([gt[m, zz] for zz in range(NZ)], axis=1),
+            jnp.concatenate([fw[m, zz].reshape(256, 256) for zz in range(NZ)], axis=0),
         )
-
-    def project(m):
-        if m == 2:
-            both = product(m, range(8))
-        else:
-            both = both_v[m] + product(m, FAR_Z)
         part = (both[:256] + both[256:]).T
         for half in range(2):
             cols = part[:, half * 128:(half + 1) * 128]
@@ -382,8 +375,6 @@
     f.ring(2, FAR_Z, "late")
     f.line_end(2, FAR_Z, "late")
     f.got("early")
-    for m in range(2):
-        both_v[m] = product(m, (0,) + NEAR_Z)
     f.exchange()
     w.far(1)
     w.cross(0)
@@ -536,7 +527,7 @@
         scratch_shapes=[
             V((1024, 2048), BF), V((3, 1024, 256), BF), V((768, 1024), BF),
             V((3, NZ, NX, 2, 4, 8, 256), BF), V((3, NZ, NX, 2, 4, 8, 256), BF), V((3 * D, 256), F32),
-            V((3, NZ, 512, 256), BF), V((3, 512, 256), F32), V((3, D, 256), F32), V((3, 32, 256), F32),
+            V((3, NZ, 512, 256), BF), V((3, D, 256), F32), V((3, 32, 256), F32),
             V((2, 2, NX, 64, 128), F32), V((2, NZ, 32, 128), F32),
             V((2, NX, 64, 128), F32), V((NZ, 32, 128), F32),
             V((2, NX, 64, 128), F32), V((NZ, 32, 128), F32),

time: 60 us -> 60.1 us (level)
  no operation moved by 1% of the time
where the time goes in v5:
time: 60.1 us
  Pallas kernels  59.4 us (99%)
  between operations  0.64 us (1%)
    pallas_call x1, Pallas kernels, local(): pl.pallas_call(kernel, out_shape=(V((3, 32, 256), F32), V((3, 32, 256), F...  57.1 us
    pallas_call x1, Pallas kernels, local(): pl.pallas_call(write_out, out_shape=tuple((jax.ShapeDtypeStruct(r.shape,...  2.33 us

profile of v5, /device:TPU:1, one launch (start us, length us, event | category | flops | bytes accessed | tf_op | source)
XLA Modules:
  0.0 60.1 jit_solution(9973837012633095754)
XLA Ops:
  0.6 57.1 %update.1 = (f32[3,32,256]{2,1,0:T(8,128)S(1)}, f32[3,32,256]{2,1,0:T(8,128)S(1)}, bf16[3,2048,256]{2,1,0:T(8,128)(2,1)S(1)}, f32[3,256,256]{2,1,0:T(8,128)S(1)}, f32[3,256,256]{2,1,0:T(8,128)S(1)}) custom-call(bf16[1024,2048]{1,0:T(8,128)(2,1)} %inputs.1, bf16[3,1024,256]{2,1,0:T(8,128)(2,1)} %bitcast.1, bf16[3,32,256]{2,1,0:T(8,128)(2,1)} %factors.1, ...), custom_call_target="tpu_custom_call" | custom-call | tf_op jit(solution)/shard_map/update/pallas_call | solution.py:520
  57.7 2.3 %write_out.1 = (f32[3,32,256]{2,1,0:T(8,128)}, f32[3,32,256]{2,1,0:T(8,128)}, bf16[3,2048,256]{2,1,0:T(8,128)(2,1)}, f32[3,256,256]{2,1,0:T(8,128)}, f32[3,256,256]{2,1,0:T(8,128)}) custom-call(f32[3,32,256]{2,1,0:T(8,128)S(1)} %get-tuple-element.10.refs_0_, f32[3,32,256]{2,1,0:T(8,128)S(1)} %get-tuple-element.11.refs_1_, ...), custom_call_target="tpu_custom_call" | custom-call | tf_op jit(solution)/shard_map/write_out/pallas_call | solution.py:546
